TPU v7x, 32 devices: a whole 2x2x4 slice. The times are simulated.
32 devices in a mesh: grp: 2 (over y), ep: 4 (over z), tp: 4 (over x, core).
Axes of the slice: x: 2, y: 2, z: 4, core: 2. Of those that a mesh axis runs over, the one named last changes fastest.
Arguments:
- query_rows: bfloat16 [1536, 2048], P(('grp', 'ep'), 'tp'), parts along dimension 0, may hold values from -100 to 100
- projected_keys: bfloat16 [1536, 512], P(('grp', 'ep'), 'tp'), parts along dimension 0, may hold values from -100 to 100
- projected_values: bfloat16 [1536, 512], P(('grp', 'ep'), 'tp'), parts along dimension 0, may hold values from -6 to 6
- query_gain: float32 [128], replicated, may hold values from 0.3 to 6.5
- key_norm_gain: float32 [128], replicated, may hold values from 0.3 to 6.5
- out_proj: bfloat16 [2048, 2048], P('tp'), may hold values from -4 to 4
- mix_tokens: bfloat16 [4096, 2048], P(('grp', 'ep', 'tp')), parts along dimension 0, may hold values from -150 to 150
- norm_gain: float32 [2048], replicated, may hold values from 0.1 to 1.9
- expert_ids: int32 [4096, 2], P(('grp', 'ep', 'tp')), parts along dimension 0, may hold values from 0 to 3, all different within a row; in each aligned block of 128 rows (0 to 127, 128 to 255, ...) at most 96 rows name the same one
- expert_score: float32 [4096, 2], P(('grp', 'ep', 'tp')), parts along dimension 0, may hold values from -6 to 6
- gate_proj: bfloat16 [4, 2048, 2048], P('ep', None, 'tp'), may hold values from -0.125 to 0.125
- up_proj: bfloat16 [4, 2048, 2048], P('ep', None, 'tp'), may hold values from -0.125 to 0.125
- down_proj: bfloat16 [4, 2048, 2048], P('ep', 'tp'), may hold values from -0.125 to 0.125
Outputs:
- mixed_rows: bfloat16 [1536, 2048], P(('grp', 'ep', 'tp')), parts along dimension 0
- expert_out: bfloat16 [4096, 2048], P(('grp', 'ep', 'tp')), parts along dimension 0
There are 2 independent parts, one for each index of `grp`. A program takes and returns all parts, laid end to end along the dimension named above; an argument that names none is the same for every part. Nothing has to cross between parts.
Inputs may be any that keep to these rules, and one draw needn't show every extreme that they name: `expert_ids`: each row names 2 different experts. Within the rows of one device (aligned blocks of 128 rows) no expert is named more than 96 times, and in every draw some device names some expert exactly 96 times.
All inputs are finite; a program needn't handle non-finite values.
Results may differ from a plain program's by a relative error of at most 0.014.
The roundings to bfloat16 on the way count: a program that leaves them out, or rounds other values in their place, can miss the bound.
Values may be sent and summed in bfloat16 or wider, within the bound.
A program may use at most 128 MiB of HBM per device.

v0:
```python
import math
import jax
import jax.numpy as jnp
from jax import lax
from jax.sharding import PartitionSpec as P

GRID_W = 64
EPS = 1e-06
THETA = 10000.0


def head_norm(vectors, gain):
    return vectors * lax.rsqrt(jnp.mean(vectors * vectors, axis=-1, keepdims=True) + EPS) * gain


def rotate_grid(vectors, token_positions):
    length, heads, head_dim = vectors.shape
    quarter = head_dim // 4
    freqs = 1.0 / THETA ** (jnp.arange(quarter, dtype=jnp.float32) * 4.0 / head_dim)
    grid_row = (token_positions // GRID_W).astype(jnp.float32)
    grid_col = (token_positions % GRID_W).astype(jnp.float32)
    angles = jnp.stack([grid_row[:, None] * freqs, grid_col[:, None] * freqs], axis=1)
    cosine = jnp.cos(angles)[:, None]
    sine = jnp.sin(angles)[:, None]
    halves = vectors.reshape(length, heads, 2, 2, quarter)
    first = halves[..., 0, :]
    second = halves[..., 1, :]
    turned = jnp.stack([first * cosine - second * sine, second * cosine + first * sine], axis=-2)
    return turned.reshape(length, heads, head_dim)


def prepare_inputs(raw_rows, gain, heads, token_positions):
    length = raw_rows.shape[0]
    head_dim = gain.shape[0]
    vectors = raw_rows.astype(jnp.float32).reshape(length, heads, head_dim)
    return rotate_grid(head_norm(vectors, gain), token_positions).astype(jnp.bfloat16)


def mixer_half(query_rows, projected_keys, projected_values, query_gain, key_norm_gain, out_proj):
    length = query_rows.shape[0]
    head_dim = query_gain.shape[0]
    kv_heads = projected_keys.shape[1] // head_dim
    q_heads = query_rows.shape[1] // head_dim
    queries_per_group = q_heads // kv_heads
    token_positions = lax.axis_index("ep") * length + jnp.arange(length, dtype=jnp.int32)
    query_matrix = prepare_inputs(query_rows, query_gain, q_heads, token_positions).reshape(
        length, kv_heads, queries_per_group, head_dim
    )
    keys_turned = prepare_inputs(projected_keys, key_norm_gain, kv_heads, token_positions).reshape(
        length, kv_heads * head_dim
    )
    score_scale = head_dim ** (-0.5)
    initial = (
        jnp.full((kv_heads, queries_per_group, length), -1e30, jnp.float32),
        jnp.zeros((kv_heads, queries_per_group, length), jnp.float32),
        jnp.zeros((length, kv_heads, queries_per_group, head_dim), jnp.float32),
    )
    key_piece = lax.all_gather(keys_turned, "ep", axis=0, tiled=True)
    value_piece = lax.all_gather(projected_values, "ep", axis=0, tiled=True)
    piece_rows = key_piece.shape[0]
    step_rows = math.gcd(piece_rows, 1024)

    def one_block(block_index, running):
        run_max, run_sum, run_acc = running
        offset = block_index * step_rows
        key_block = lax.dynamic_slice_in_dim(key_piece, offset, step_rows, 0).reshape(
            step_rows, kv_heads, head_dim
        )
        value_block = lax.dynamic_slice_in_dim(value_piece, offset, step_rows, 0).reshape(
            step_rows, kv_heads, head_dim
        )
        scores = (
            jnp.einsum(
                "tkgd,skd->kgts", query_matrix, key_block, preferred_element_type=jnp.float32
            )
            * score_scale
        )
        new_max = jnp.maximum(run_max, jnp.max(scores, axis=-1))
        factor = jnp.exp(run_max - new_max)
        weights = jnp.exp(scores - new_max[..., None])
        run_sum = run_sum * factor + jnp.sum(weights, axis=-1)
        update = jnp.einsum(
            "kgts,skd->tkgd",
            weights.astype(jnp.bfloat16),
            value_block,
            preferred_element_type=jnp.float32,
        )
        run_acc = run_acc * jnp.transpose(factor, (2, 0, 1))[..., None] + update
        return (new_max, run_sum, run_acc)

    run_max, run_sum, run_acc = lax.fori_loop(0, piece_rows // step_rows, one_block, initial)
    heads_out = (
        (run_acc / jnp.transpose(run_sum, (2, 0, 1))[..., None])
        .astype(jnp.bfloat16)
        .reshape(length, q_heads * head_dim)
    )
    return lax.psum_scatter(
        jnp.dot(heads_out, out_proj, preferred_element_type=jnp.float32).astype(jnp.bfloat16),
        "tp",
        scatter_dimension=0,
        tiled=True,
    )


def expert_half(mix_tokens, norm_gain, expert_ids, expert_score, gate_proj, up_proj, down_proj):
    length, model_dim = mix_tokens.shape
    top_count = expert_ids.shape[1]
    local_experts = gate_proj.shape[0]
    expert_axis = lax.axis_size("ep")
    experts_all = expert_axis * local_experts
    capacity = length * top_count * 3 // (2 * experts_all)
    values_b = mix_tokens.astype(jnp.float32)
    normed = (
        values_b
        * lax.rsqrt(jnp.mean(values_b * values_b, axis=-1, keepdims=True) + EPS)
        * norm_gain
    ).astype(jnp.bfloat16)
    flat = expert_ids.reshape(length * top_count)
    onehot = (flat[:, None] == jnp.arange(experts_all, dtype=jnp.int32)).astype(jnp.int32)
    slots = jnp.sum((jnp.cumsum(onehot, axis=0) - onehot) * onehot, axis=1)
    target = flat * capacity + slots
    placed = (target[:, None] == jnp.arange(experts_all * capacity, dtype=jnp.int32)).astype(
        jnp.int32
    )
    placed = jnp.sum(placed.reshape(length, top_count, experts_all * capacity), axis=1).astype(
        jnp.bfloat16
    )
    outgoing = jnp.einsum("re,rd->ed", placed, normed, preferred_element_type=jnp.float32).astype(
        jnp.bfloat16
    )
    outgoing = outgoing.reshape(expert_axis, local_experts, capacity, model_dim)
    rows_in = lax.all_gather(
        lax.all_to_all(outgoing, "ep", split_axis=0, concat_axis=0, tiled=True),
        "tp",
        axis=0,
        tiled=True,
    )
    gate_out = jnp.einsum("secd,edf->secf", rows_in, gate_proj, preferred_element_type=jnp.float32)
    up_out = jnp.einsum("secd,edf->secf", rows_in, up_proj, preferred_element_type=jnp.float32)
    active = (jax.nn.silu(gate_out) * up_out).astype(jnp.bfloat16)
    summed = lax.psum_scatter(
        jnp.einsum("secf,efd->secd", active, down_proj, preferred_element_type=jnp.float32).astype(
            jnp.bfloat16
        ),
        "tp",
        scatter_dimension=0,
        tiled=True,
    )
    returned = lax.all_to_all(summed, "ep", split_axis=0, concat_axis=0, tiled=True)
    results = returned.reshape(experts_all * capacity, model_dim)
    selected_expert = target.reshape(length, top_count)
    first_weight = jax.nn.sigmoid(expert_score[:, 0] - expert_score[:, 1])
    combined = first_weight[:, None] * results[selected_expert[:, 0]].astype(jnp.float32) + (
        1.0 - first_weight
    )[:, None] * results[selected_expert[:, 1]].astype(jnp.float32)
    return combined.astype(jnp.bfloat16)


def local(
    query_rows,
    projected_keys,
    projected_values,
    query_gain,
    key_norm_gain,
    out_proj,
    mix_tokens,
    norm_gain,
    expert_ids,
    expert_score,
    gate_proj,
    up_proj,
    down_proj,
):
    mixed_rows = mixer_half(
        query_rows, projected_keys, projected_values, query_gain, key_norm_gain, out_proj
    )
    expert_out = expert_half(
        mix_tokens, norm_gain, expert_ids, expert_score, gate_proj, up_proj, down_proj
    )
    return (mixed_rows, expert_out)


def solution(mesh):
    in_specs = (
        P(("grp", "ep"), "tp"),
        P(("grp", "ep"), "tp"),
        P(("grp", "ep"), "tp"),
        P(),
        P(),
        P("tp", None),
        P(("grp", "ep", "tp"), None),
        P(),
        P(("grp", "ep", "tp"), None),
        P(("grp", "ep", "tp"), None),
        P("ep", None, "tp"),
        P("ep", None, "tp"),
        P("ep", "tp", None),
    )
    out_specs = (P(("grp", "ep", "tp"), None), P(("grp", "ep", "tp"), None))
    return jax.shard_map(local, mesh=mesh, in_specs=in_specs, out_specs=out_specs, check_vma=False)
```

profile of v0, /device:TPU:0, one launch (start us, length us, event | category | flops | bytes accessed | tf_op | source)
XLA Modules:
  0.0 237.6 jit_solution(8891725918785150637)
XLA Ops:
  7.2 0.9 copy.76
  8.2 0.1 eq.46
  8.3 0.1 eq.42
  8.4 1.2 reduce-window.6
  9.7 0.1 copy.78
  9.9 0.1 copy.79
  10.1 0.1 reduce_sum.63
  10.3 0.7 multiply_add_fusion
  11.0 0.1 convert_reduce_fusion
  11.1 1.2 fusion.39
  12.3 1.7 convolution_convert_fusion
  14.1 43.2 %all_to_all.10 = bf16[4,1,96,2048]{3,2,1,0:T(8,128)(2,1)} all-to-all(bf16[4,1,96,2048]{3,2,1,0:T(8,128)(2,1)S(1)} %bitcast.175), channel_id=1, replica_groups=mesh['grp'=2,'ep'=4,'tp'=4] {'ep'}, dimensions={0} | all-to-all | bytes 3145728 | tf_op jit(solution)/shard_map/all_to_all | solution.py:133
  57.4 45.6 %all-gather.2.cloned.1.call-done = bf16[16,1,96,2048]{3,2,1,0:T(8,128)(2,1)} async-done(((bf16[4,1,96,2048]{3,2,1,0:T(8,128)(2,1)}), bf16[16,1,96,2048]{3,2,1,0:T(8,128)(2,1)}) %all-gather.2.cloned.1.call-update) | async-done | bytes 6291472 | tf_op jit(solution)/shard_map/all_gather | solution.py:132
  103.0 8.5 %fusion.15 = f32[16,96,512]{2,1,0:T(8,128)} fusion(bf16[16,1,96,2048]{3,2,1,0:T(8,128)(2,1)} %all-gather.2.cloned.1.call-done, bf16[1,2048,512]{2,1,0:T(8,128)(2,1)} %param.26), kind=kOutput, calls=%fused_computation.24 | convolution fusion | flops 3221225472 | bytes 11534336 | tf_op jit(solution)/shard_map/secd,edf->secf/dot_general | solution.py:139
  111.5 11.9 %convert_bitcast_fusion = bf16[16,1,96,2048]{3,2,0,1:T(8,128)(2,1)} fusion(bf16[1,512,2048]{2,1,0:T(8,128)(2,1)S(1)} %copy-done, f32[16,96,512]{2,1,0:T(8,128)} %fusion.15, bf16[1,2048,512]{2,1,0:T(8,128)(2,1)} %param.25, bf16[16,1,96,2048]{3,2,1,0:T(8,128)(2,1)} %all-gather.2.cloned.1.call-done), kind=kOutput, calls=%fused_computation.28 | convolution fusion | flops 6450315264 | bytes 19922944 | tf_op jit(solution)/shard_map/secf,efd->secd/dot_general | solution.py:142
  123.5 0.8 copy-done.1
  124.3 0.1 copy.73
  124.5 0.1 mul.316
  124.6 0.1 broadcast_multiply_fusion.1
  124.7 0.2 fusion.51
  125.0 0.1 multiply_multiply_fusion
  125.1 0.1 subtract_convert_fusion
  125.3 0.2 copy.74
  125.4 0.1 copy.71
  125.6 0.1 fusion.48
  125.7 0.3 subtract_convert_fusion.1
  126.0 0.1 copy.72
  126.1 14.4 %all_gather.9 = bf16[768,128]{1,0:T(8,128)(2,1)} all-gather(bf16[192,128]{1,0:T(8,128)(2,1)S(1)} %copy.72), channel_id=1, replica_groups=mesh['grp'=2,'ep'=4,'tp'=4] {'ep'}, dimensions={0}, use_global_device_ids=true | all-gather | bytes 245760 | tf_op jit(solution)/shard_map/all_gather | solution.py:58
  140.5 14.8 %all_gather.10 = bf16[768,128]{1,0:T(8,128)(2,1)} all-gather(bf16[192,128]{1,0:T(8,128)(2,1)S(1)} %copy-done.3), channel_id=1, replica_groups=mesh['grp'=2,'ep'=4,'tp'=4] {'ep'}, dimensions={0}, use_global_device_ids=true | all-gather | bytes 245760 | tf_op jit(solution)/shard_map/all_gather | solution.py:59
  155.2 27.2 %reduce-scatter.5.cloned.1.call-done = bf16[4,1,96,2048]{3,2,0,1:T(8,128)(2,1)} async-done(((bf16[16,1,96,2048]{3,2,0,1:T(8,128)(2,1)}), bf16[4,1,96,2048]{3,2,0,1:T(8,128)(2,1)}) %reduce-scatter.5.cloned.1.call-update) | async-done | bytes 1572880 | tf_op jit(solution)/shard_map/reduce_scatter | solution.py:141
  182.4 4.6 %all-to-all-start.1 = ((bf16[4,1,96,2048]{3,2,1,0:T(8,128)(2,1)}), bf16[4,1,96,2048]{3,2,1,0:T(8,128)(2,1)}, u32[]{:S(2)}, u32[]{:S(2)}) async-start(bf16[4,1,96,2048]{3,2,1,0:T(8,128)(2,1)} %bitcast.179), calls=%async_computation.3 | async-start | bytes 3145728 | tf_op jit(solution)/shard_map/all_to_all | solution.py:149
  187.0 8.8 %while.18 = (s32[]{:T(128)}, f32[1,4,192]{2,1,0:T(4,128)S(1)}, f32[1,4,192]{2,1,0:T(4,128)S(1)}, f32[192,1,4,128]{3,0,2,1:T(8,128)S(1)}, bf16[768,128]{1,0:T(8,1...) while((s32[]{:T(128)}, f32[1,4,192]{2,1,0:T(4,128)S(1)}, ...), condition=%wide.region_5.6_spmd.clone, body=%wide.region_2.5_spmd.clone.sunk | while | flops 102142472 | bytes 3522735 | solution.py:91
  187.0 1.2 fusion.75
  188.3 1.2 fusion.78
  189.5 0.4 fusion.77
  189.9 1.3 fusion.75
  191.2 1.2 fusion.78
  192.5 0.4 fusion.77
  192.9 1.3 fusion.75
  194.2 1.2 fusion.78
  195.4 0.4 fusion.77
  195.8 0.2 divide_convert_fusion
  196.0 0.2 copy.75
  196.2 3.1 %convolution_convert_fusion.1 = bf16[192,2048]{1,0:T(8,128)(2,1)} fusion(bf16[512,2048]{1,0:T(8,128)(2,1)} %param.20, bf16[24,8,4,128]{3,2,1,0:T(4,128)(2,1)S(1)} %bitcast.181), kind=kOutput, calls=%fused_computation.37 | convolution fusion | flops 403046400 | bytes 3080192 | tf_op jit(solution)/shard_map/dot_general | solution.py:98
  199.3 24.6 %all-to-all-done.1 = bf16[4,1,96,2048]{3,2,1,0:T(8,128)(2,1)} async-done(((bf16[4,1,96,2048]{3,2,1,0:T(8,128)(2,1)}), bf16[4,1,96,2048]{3,2,1,0:T(8,128)(2,1)}, u32[]{:S(2)}, u32[]{:S(2)}) %all-to-all-start.1) | async-done | bytes 1572896 | tf_op jit(solution)/shard_map/all_to_all | solution.py:149
  223.9 3.0 %gather_fusion = bf16[128,2048]{1,0:T(8,128)(2,1)S(1)} fusion(bf16[384,2048]{1,0:T(8,128)(2,1)} %bitcast.34, s32[1024]{0:T(1024)S(1)} %get-tuple-element.225), kind=kCustom, calls=%fused_computation | custom fusion | bytes 1049088 | tf_op jit(solution)/shard_map/gather | solution.py:153
  227.0 3.1 %gather_fusion.1 = bf16[128,2048]{1,0:T(8,128)(2,1)S(1)} fusion(bf16[384,2048]{1,0:T(8,128)(2,1)} %bitcast.34, s32[1024]{0:T(1024)S(1)} %get-tuple-element.224), kind=kCustom, calls=%fused_computation.1 | custom fusion | bytes 1049088 | tf_op jit(solution)/shard_map/gather | solution.py:155
  230.0 1.0 add_convert_fusion
  (51 shorter events, 0.8 us)
Async XLA Ops:
  7.2 104.3 %copy-start = (bf16[1,512,2048]{2,1,0:T(8,128)(2,1)S(1)}, bf16[1,512,2048]{2,1,0:T(8,128)(2,1)}, u32[]{:S(2)}) copy-start(bf16[1,512,2048]{2,1,0:T(8,128)(2,1)} %param.27) | copy-start | bytes 6291460
  7.2 95.8 %all-gather.2.cloned.1.call-start = ((), (), s32[]{:S(2)}) async-start(), calls=%async_computation.5 | async-start | bytes 7864320 | tf_op jit(solution)/shard_map/all_gather | solution.py:132
  57.3 125.1 %reduce-scatter.5.cloned.1.call-start = ((), (), s32[]{:S(2)}) async-start(), calls=%async_computation.6 | async-start | bytes 7864320 | tf_op jit(solution)/shard_map/reduce_scatter | solution.py:141
  123.4 0.9 copy-start.1
  123.4 1.1 copy-start.6
  123.4 2.0 copy-start.2
  123.4 2.2 copy-start.5
  124.9 15.6 %copy-start.3 = (bf16[192,128]{1,0:T(8,128)(2,1)S(1)}, bf16[192,128]{1,0:T(8,128)(2,1)}, u32[]{:S(2)}) copy-start(bf16[192,128]{1,0:T(8,128)(2,1)} %param.17) | copy-start | bytes 147460
  182.4 41.5 %all-to-all-start.1 = ((bf16[4,1,96,2048]{3,2,1,0:T(8,128)(2,1)}), bf16[4,1,96,2048]{3,2,1,0:T(8,128)(2,1)}, u32[]{:S(2)}, u32[]{:S(2)}) async-start(bf16[4,1,96,2048]{3,2,1,0:T(8,128)(2,1)} %bitcast.179), calls=%async_computation.3 | async-start | bytes 3145728 | tf_op jit(solution)/shard_map/all_to_all | solution.py:149
  187.0 44.1 %reduce-scatter.3.cloned.1.call-start = ((), (), s32[]{:S(2)}) async-start(), calls=%async_computation.4 | async-start | bytes 983040 | tf_op jit(solution)/shard_map/reduce_scatter | solution.py:97
  196.0 3.3 %copy-start.4 = (f32[128,2]{0,1:T(2,128)S(1)}, f32[128,2]{0,1:T(2,128)}, u32[]{:S(2)}) copy-start(f32[128,2]{0,1:T(2,128)} %param.24) | copy-start | bytes 3076
Sparse Core Ops, SparseCore 0:
  57.4 45.4 all-gather.1
  123.5 58.8 reduce-scatter.4
  199.4 23.6 reduce-scatter.2
where the time goes:
time: 238 us
  waiting for transfers between devices  97.5 us (41%)
  blocking collectives  72.3 us (30%)
  matrix products  32.6 us (14%)
  between operations  14 us (6%)
  local copies, waits for them, and re-layouts  9.41 us (4%)
  other arithmetic  6.92 us (3%)
  starting transfers between devices  4.68 us (2%)
    all_gather x1, waiting for transfers between devices, expert_half(): lax.all_gather(lax.all_to_all(outgoing, 'ep', split_axis=0, concat_axis=0...  45.6 us
    all_to_all x1, blocking collectives, expert_half(): lax.all_to_all(outgoing, 'ep', split_axis=0, concat_axis=0, tiled=True)  43.2 us
    reduce_scatter x1, waiting for transfers between devices, expert_half(): lax.psum_scatter(jnp.einsum('secf,efd->secd', active, down_proj, preferre...  27.2 us
    all_to_all x1, waiting for transfers between devices, expert_half(): lax.all_to_all(summed, 'ep', split_axis=0, concat_axis=0, tiled=True)  24.6 us
    all_gather x1, blocking collectives, mixer_half(): value_piece = lax.all_gather(projected_values, 'ep', axis=0, tiled=True)  14.8 us
    all_gather x1, blocking collectives, mixer_half(): key_piece = lax.all_gather(keys_turned, 'ep', axis=0, tiled=True)  14.4 us
    dot_general x1, matrix products, expert_half(): jnp.einsum('secf,efd->secd', active, down_proj, preferred_element_type=jn...  11.9 us
    dot_general x1, matrix products, expert_half(): jnp.einsum('secd,edf->secf', rows_in, up_proj, preferred_element_type=jnp...  8.52 us
  transfers between devices with their start and end apart: 4, of which 3 were waited for; matrix products, arithmetic and copies ran while one was open for 9% of the time, Pallas kernels for 0%

commit v1 on v0

--- a/solution.py
+++ b/solution.py
@@ -7,6 +7,22 @@
 GRID_W = 64
 EPS = 1e-06
 THETA = 10000.0
+
+
+def exchange_in_pairs(shard, axis, split, join):
+    ways, here = (lax.axis_size(axis), lax.axis_index(axis))
+    width = shard.shape[split] // ways
+    shape = list(shard.shape)
+    shape[split] = width
+    height = shape[join]
+    shape[join] = height * ways
+    full = jnp.zeros(shape, shard.dtype)
+    for mask in range(ways):
+        part = lax.dynamic_slice_in_dim(shard, (here ^ mask) * width, width, axis=split)
+        if mask:
+            part = lax.ppermute(part, axis, [(d, d ^ mask) for d in range(ways)])
+        full = lax.dynamic_update_slice_in_dim(full, part, (here ^ mask) * height, axis=join)
+    return full
 
 
 def head_norm(vectors, gain):
@@ -146,7 +162,7 @@
         scatter_dimension=0,
         tiled=True,
     )
-    returned = lax.all_to_all(summed, "ep", split_axis=0, concat_axis=0, tiled=True)
+    returned = exchange_in_pairs(summed, "ep", 0, 0)
     results = returned.reshape(experts_all * capacity, model_dim)
     selected_expert = target.reshape(length, top_count)
     first_weight = jax.nn.sigmoid(expert_score[:, 0] - expert_score[:, 1])

time: 238 us -> 236 us (level); the launches traced: 238 us -> 232 us
  waiting for transfers between devices: 97.5 us -> 86.3 us
  local copies, waits for them, and re-layouts: 9.41 us -> 14.6 us
    ppermute x0 -> x3, waiting for transfers between devices: none -> 26 us  [exchange_in_pairs(): part = lax.ppermute(part, axis, [(d, d ^ mask) for d in range(ways)])]
    all_to_all x1 -> x0, waiting for transfers between devices: 24.6 us -> none  [expert_half(): lax.all_to_all(summed, 'ep', split_axis=0, concat_axis=0, tiled=True)]
    reduce_scatter x1, waiting for transfers between devices: 27.2 us -> 14.7 us  [expert_half(): lax.psum_scatter(jnp.einsum('secf,efd->secd', active, down_proj, preferre...]
    all_to_all x1 -> x0, starting transfers between devices: 4.59 us -> none  [expert_half(): lax.all_to_all(summed, 'ep', split_axis=0, concat_axis=0, tiled=True)]
    ppermute x0 -> x3, starting transfers between devices: none -> 4.45 us  [exchange_in_pairs(): part = lax.ppermute(part, axis, [(d, d ^ mask) for d in range(ways)])]
  transfers between devices with their start and end apart: 4 -> 6, of which waited for: 3 -> 4; matrix products, arithmetic and copies ran while one was open for 9% -> 11% of each run, Pallas kernels for 0% -> 0%
where the time goes in v1:
time: 236 us; the launch traced here: 232 us
  waiting for transfers between devices  86.3 us (37%)
  blocking collectives  72.5 us (31%)
  matrix products  32.7 us (14%)
  local copies, waits for them, and re-layouts  14.6 us (6%)
  between operations  14 us (6%)
  other arithmetic  6.93 us (3%)
  starting transfers between devices  4.57 us (2%)
    all_gather x1, waiting for transfers between devices, expert_half(): lax.all_gather(lax.all_to_all(outgoing, 'ep', split_axis=0, concat_axis=0...  45.6 us
    all_to_all x1, blocking collectives, expert_half(): lax.all_to_all(outgoing, 'ep', split_axis=0, concat_axis=0, tiled=True)  43.2 us
    ppermute x3, waiting for transfers between devices, exchange_in_pairs(): part = lax.ppermute(part, axis, [(d, d ^ mask) for d in range(ways)])  26 us
    all_gather x1, blocking collectives, mixer_half(): value_piece = lax.all_gather(projected_values, 'ep', axis=0, tiled=True)  14.9 us
    reduce_scatter x1, waiting for transfers between devices, expert_half(): lax.psum_scatter(jnp.einsum('secf,efd->secd', active, down_proj, preferre...  14.7 us
    all_gather x1, blocking collectives, mixer_half(): key_piece = lax.all_gather(keys_turned, 'ep', axis=0, tiled=True)  14.4 us
    dot_general x1, matrix products, expert_half(): jnp.einsum('secf,efd->secd', active, down_proj, preferred_element_type=jn...  11.9 us
    dot_general x1, matrix products, expert_half(): jnp.einsum('secd,edf->secf', rows_in, up_proj, preferred_element_type=jnp...  8.52 us
  transfers between devices with their start and end apart: 6, of which 4 were waited for; matrix products, arithmetic and copies ran while one was open for 11% of the time, Pallas kernels for 0%

profile of v1, /device:TPU:0, one launch (start us, length us, event | category | flops | bytes accessed | tf_op | source)
XLA Modules:
  0.0 231.8 jit_solution(18405090323270470741)
XLA Ops:
  7.2 0.9 copy.74
  8.2 0.1 eq.46
  8.3 0.1 eq.42
  8.4 1.2 reduce-window.6
  10.1 0.1 reduce_sum.63
  10.3 0.7 multiply_add_fusion
  11.1 1.2 fusion.39
  12.3 1.7 convolution_convert_fusion
  14.1 43.2 %all_to_all.5 = bf16[4,1,96,2048]{3,2,1,0:T(8,128)(2,1)} all-to-all(bf16[4,1,96,2048]{3,2,1,0:T(8,128)(2,1)S(1)} %bitcast.174), channel_id=1, replica_groups=mesh['grp'=2,'ep'=4,'tp'=4] {'ep'}, dimensions={0} | all-to-all | bytes 3145728 | tf_op jit(solution)/shard_map/all_to_all | solution.py:149
  57.4 45.6 %all-gather.2.cloned.1.call-done = bf16[16,1,96,2048]{3,2,1,0:T(8,128)(2,1)} async-done(((bf16[4,1,96,2048]{3,2,1,0:T(8,128)(2,1)}), bf16[16,1,96,2048]{3,2,1,0:T(8,128)(2,1)}) %all-gather.2.cloned.1.call-update) | async-done | bytes 6291472 | tf_op jit(solution)/shard_map/all_gather | solution.py:148
  103.0 8.5 %fusion.15 = f32[16,96,512]{2,1,0:T(8,128)} fusion(bf16[16,1,96,2048]{3,2,1,0:T(8,128)(2,1)} %all-gather.2.cloned.1.call-done, bf16[1,2048,512]{2,1,0:T(8,128)(2,1)} %param.26), kind=kOutput, calls=%fused_computation.24 | convolution fusion | flops 3221225472 | bytes 11534336 | tf_op jit(solution)/shard_map/secd,edf->secf/dot_general | solution.py:155
  111.5 11.9 %convert_bitcast_fusion = bf16[16,1,96,2048]{3,2,0,1:T(8,128)(2,1)} fusion(bf16[1,512,2048]{2,1,0:T(8,128)(2,1)S(1)} %copy-done, f32[16,96,512]{2,1,0:T(8,128)} %fusion.15, bf16[1,2048,512]{2,1,0:T(8,128)(2,1)} %param.25, bf16[16,1,96,2048]{3,2,1,0:T(8,128)(2,1)} %all-gather.2.cloned.1.call-done), kind=kOutput, calls=%fused_computation.28 | convolution fusion | flops 6450315264 | bytes 19922944 | tf_op jit(solution)/shard_map/secf,efd->secd/dot_general | solution.py:158
  123.5 0.8 copy-done.2
  124.3 0.1 copy.71
  124.7 0.2 fusion.51
  125.3 0.2 copy.72
  125.5 0.1 copy.69
  125.7 0.3 subtract_convert_fusion.1
  126.1 14.4 %all_gather.9 = bf16[768,128]{1,0:T(8,128)(2,1)} all-gather(bf16[192,128]{1,0:T(8,128)(2,1)S(1)} %copy.70), channel_id=1, replica_groups=mesh['grp'=2,'ep'=4,'tp'=4] {'ep'}, dimensions={0}, use_global_device_ids=true | all-gather | bytes 245760 | tf_op jit(solution)/shard_map/all_gather | solution.py:74
  140.5 14.9 %all_gather.10 = bf16[768,128]{1,0:T(8,128)(2,1)} all-gather(bf16[192,128]{1,0:T(8,128)(2,1)S(1)} %copy-done.4), channel_id=1, replica_groups=mesh['grp'=2,'ep'=4,'tp'=4] {'ep'}, dimensions={0}, use_global_device_ids=true | all-gather | bytes 245760 | tf_op jit(solution)/shard_map/all_gather | solution.py:75
  155.4 8.8 %while.18 = (s32[]{:T(128)}, f32[1,4,192]{2,1,0:T(4,128)S(1)}, f32[1,4,192]{2,1,0:T(4,128)S(1)}, f32[192,1,4,128]{3,0,2,1:T(8,128)S(1)}, bf16[768,128]{1,0:T(8,1...) while((s32[]{:T(128)}, f32[1,4,192]{2,1,0:T(4,128)S(1)}, ...), condition=%wide.region_5.6_spmd.clone, body=%wide.region_2.5_spmd.clone.sunk | while | flops 102142472 | bytes 3522735 | solution.py:107
  155.4 1.2 fusion.75
  156.7 1.2 fusion.78
  157.9 0.4 fusion.77
  158.3 1.2 fusion.75
  159.6 1.2 fusion.78
  160.8 0.4 fusion.77
  161.3 1.3 fusion.75
  162.5 1.2 fusion.78
  163.8 0.4 fusion.77
  164.2 0.2 divide_convert_fusion
  164.4 0.2 copy.73
  164.5 3.2 %convolution_convert_fusion.1 = bf16[192,2048]{1,0:T(8,128)(2,1)} fusion(bf16[512,2048]{1,0:T(8,128)(2,1)} %param.20, bf16[24,8,4,128]{3,2,1,0:T(4,128)(2,1)S(1)} %bitcast.179), kind=kOutput, calls=%fused_computation.37 | convolution fusion | flops 403046400 | bytes 3080192 | tf_op jit(solution)/shard_map/dot_general | solution.py:114
  167.8 14.7 %reduce-scatter.5.cloned.1.call-done = bf16[4,1,96,2048]{3,2,0,1:T(8,128)(2,1)} async-done(((bf16[16,1,96,2048]{3,2,0,1:T(8,128)(2,1)}), bf16[4,1,96,2048]{3,2,0,1:T(8,128)(2,1)}) %reduce-scatter.5.cloned.1.call-update) | async-done | bytes 1572880 | tf_op jit(solution)/shard_map/reduce_scatter | solution.py:157
  182.4 1.3 broadcast_in_dim.15
  183.8 0.6 copy-done.1
  184.4 0.9 constant_dynamic-slice_fusion
  185.3 1.5 collective-permute-start
  186.8 2.4 %collective-permute-start.1 = (bf16[1,1,96,2048]{3,2,0,1:T(8,128)(2,1)S(1)}, bf16[1,1,96,2048]{3,2,0,1:T(8,128)(2,1)S(1)}, u32[]{:S(2)}, u32[]{:S(2)}) collective-permute-start(bf16[1,1,96,2048]{3,2,0,1:T(8,128)(2,1)S(1)} %get-tuple-element.209), channel_id=1, source_target_pairs={{0,8},{4,12},{8,0},{12,4},{1,9},{5,13},{9,1},{13,5},{2,10},{6,14},... | collective-permute-start | bytes 1179656 | tf_op jit(solution)/shard_map/ppermute | solution.py:23
  189.3 0.5 collective-permute-start.2
  189.8 13.7 %collective-permute-done = bf16[1,1,96,2048]{3,2,0,1:T(8,128)(2,1)S(1)} collective-permute-done((bf16[1,1,96,2048]{3,2,0,1:T(8,128)(2,1)S(1)}, bf16[1,1,96,2048]{3,2,0,1:T(8,128)(2,1)S(1)}, u32[]{:S(2)}, u32[]{:S(2)}) %collective-permute-start) | collective-permute-done | bytes 393248 | tf_op jit(solution)/shard_map/ppermute | solution.py:23
  203.5 0.8 constant_dynamic-update-slice_fusion.1
  204.3 12.2 %collective-permute-done.1 = bf16[1,1,96,2048]{3,2,0,1:T(8,128)(2,1)S(1)} collective-permute-done((bf16[1,1,96,2048]{3,2,0,1:T(8,128)(2,1)S(1)}, bf16[1,1,96,2048]{3,2,0,1:T(8,128)(2,1)S(1)}, u32[]{:S(2)}, u32[]{:S(2)}) %collective-permute-start.1) | collective-permute-done | bytes 393248 | tf_op jit(solution)/shard_map/ppermute | solution.py:23
  216.6 0.8 constant_dynamic-update-slice_fusion
  217.3 0.8 constant_dynamic-update-slice_fusion.2
  218.1 3.0 %gather_fusion = bf16[128,2048]{1,0:T(8,128)(2,1)S(1)} fusion(bf16[384,2048]{1,0:T(8,128)(2,1)} %bitcast.33, s32[1024]{0:T(1024)S(1)} %get-tuple-element.229), kind=kCustom, calls=%fused_computation | custom fusion | bytes 1049088 | tf_op jit(solution)/shard_map/gather | solution.py:169
  221.2 3.1 %gather_fusion.1 = bf16[128,2048]{1,0:T(8,128)(2,1)S(1)} fusion(bf16[384,2048]{1,0:T(8,128)(2,1)} %bitcast.33, s32[1024]{0:T(1024)S(1)} %get-tuple-element.228), kind=kCustom, calls=%fused_computation.1 | custom fusion | bytes 1049088 | tf_op jit(solution)/shard_map/gather | solution.py:171
  224.3 1.0 add_convert_fusion
  (62 shorter events, 1.7 us)
Async XLA Ops:
  7.2 104.3 %copy-start = (bf16[1,512,2048]{2,1,0:T(8,128)(2,1)S(1)}, bf16[1,512,2048]{2,1,0:T(8,128)(2,1)}, u32[]{:S(2)}) copy-start(bf16[1,512,2048]{2,1,0:T(8,128)(2,1)} %param.27) | copy-start | bytes 6291460
  7.2 95.8 %all-gather.2.cloned.1.call-start = ((), (), s32[]{:S(2)}) async-start(), calls=%async_computation.4 | async-start | bytes 7864320 | tf_op jit(solution)/shard_map/all_gather | solution.py:148
  57.3 125.1 %reduce-scatter.5.cloned.1.call-start = ((), (), s32[]{:S(2)}) async-start(), calls=%async_computation.5 | async-start | bytes 7864320 | tf_op jit(solution)/shard_map/reduce_scatter | solution.py:157
  123.4 0.9 copy-start.2
  123.4 1.1 copy-start.7
  123.4 2.0 copy-start.3
  123.4 2.2 copy-start.6
  123.5 101.8 %reduce-scatter.3.cloned.1.call-start = ((), (), s32[]{:S(2)}) async-start(), calls=%async_computation.3 | async-start | bytes 983040 | tf_op jit(solution)/shard_map/reduce_scatter | solution.py:113
  124.9 15.6 %copy-start.4 = (bf16[192,128]{1,0:T(8,128)(2,1)S(1)}, bf16[192,128]{1,0:T(8,128)(2,1)}, u32[]{:S(2)}) copy-start(bf16[192,128]{1,0:T(8,128)(2,1)} %param.17) | copy-start | bytes 147460
  182.4 2.0 copy-start.1
  182.4 6.8 %copy-start.5 = (f32[128,2]{0,1:T(2,128)S(1)}, f32[128,2]{0,1:T(2,128)}, u32[]{:S(2)}) copy-start(f32[128,2]{0,1:T(2,128)} %param.24) | copy-start | bytes 3076
  185.3 18.2 %collective-permute-start = (bf16[1,1,96,2048]{3,2,0,1:T(8,128)(2,1)S(1)}, bf16[1,1,96,2048]{3,2,0,1:T(8,128)(2,1)S(1)}, u32[]{:S(2)}, u32[]{:S(2)}) collective-permute-start(bf16[1,1,96,2048]{3,2,0,1:T(8,128)(2,1)S(1)} %get-tuple-element.210), channel_id=1, source_target_pairs={{0,4},{4,0},{8,12},{12,8},{1,5},{5,1},{9,13},{13,9},{2,6},{6,2},{1... | collective-permute-start | bytes 1179656 | tf_op jit(solution)/shard_map/ppermute | solution.py:23
  186.8 29.7 %collective-permute-start.1 = (bf16[1,1,96,2048]{3,2,0,1:T(8,128)(2,1)S(1)}, bf16[1,1,96,2048]{3,2,0,1:T(8,128)(2,1)S(1)}, u32[]{:S(2)}, u32[]{:S(2)}) collective-permute-start(bf16[1,1,96,2048]{3,2,0,1:T(8,128)(2,1)S(1)} %get-tuple-element.209), channel_id=1, source_target_pairs={{0,8},{4,12},{8,0},{12,4},{1,9},{5,13},{9,1},{13,5},{2,10},{6,14},... | collective-permute-start | bytes 1179656 | tf_op jit(solution)/shard_map/ppermute | solution.py:23
  189.3 28.1 %collective-permute-start.2 = (bf16[1,1,96,2048]{3,2,0,1:T(8,128)(2,1)S(1)}, bf16[1,1,96,2048]{3,2,0,1:T(8,128)(2,1)S(1)}, u32[]{:S(2)}, u32[]{:S(2)}) collective-permute-start(bf16[1,1,96,2048]{3,2,0,1:T(8,128)(2,1)S(1)} %get-tuple-element.208), channel_id=1, source_target_pairs={{0,12},{4,8},{8,4},{12,0},{1,13},{5,9},{9,5},{13,1},{2,14},{6,10},... | collective-permute-start | bytes 1179656 | tf_op jit(solution)/shard_map/ppermute | solution.py:23
Sparse Core Ops, SparseCore 0:
  57.4 45.4 all-gather.1
  123.5 58.8 reduce-scatter.4
  185.5 23.2 reduce-scatter.2
